TPU v7x, 32 devices: a whole 2x2x4 slice. The times are simulated.
32 devices in a mesh: sp: 16 (over z, y, x), tp: 2 (over core).
Axes of the slice: x: 2, y: 2, z: 4, core: 2. Of those that a mesh axis runs over, the one named last changes fastest.
Arguments:
- residual_in: bfloat16 [4096, 2048], P(('sp', 'tp')), may hold values from -6 to 6
- query_lean: bfloat16 [4096, 8, 96], P('sp', 'tp'), may hold values from -60 to 60
- query_broad: bfloat16 [4096, 8, 160], P('sp', 'tp'), may hold values from -60 to 60
- latent: bfloat16 [4096, 256], P('sp'), may hold values from -6 to 6
- rope_key: bfloat16 [4096, 32], P('sp'), may hold values from -8 to 8
- latent_gain: float32 [256], replicated, may hold values from 0.1 to 1.9
- key_up_lean: bfloat16 [256, 8, 64], P(None, 'tp'), may hold values from -0.375 to 0.375
- key_up_broad: bfloat16 [256, 8, 128], P(None, 'tp'), may hold values from -0.375 to 0.375
- value_up_lean: bfloat16 [256, 8, 64], P(None, 'tp'), may hold values from -0.375 to 0.375
- value_up_broad: bfloat16 [256, 8, 128], P(None, 'tp'), may hold values from -0.375 to 0.375
- out_lean: bfloat16 [8, 64, 2048], P('tp'), may hold values from -0.15625 to 0.15625
- out_broad: bfloat16 [8, 128, 2048], P('tp'), may hold values from -0.15625 to 0.15625
- attn_gain: float32 [2048], replicated, may hold values from 0.1 to 1.9
- mlp_gain: float32 [2048], replicated, may hold values from 0.1 to 1.9
- gate_weight: bfloat16 [2048, 2816], P('sp', 'tp'), may hold values from -0.125 to 0.125
- up_weight: bfloat16 [2048, 2816], P('sp', 'tp'), may hold values from -0.125 to 0.125
- down_weight: bfloat16 [2816, 2048], P('tp', 'sp'), may hold values from -0.109375 to 0.109375
Outputs:
- layer_out: bfloat16 [4096, 2048], P(('sp', 'tp'))
All inputs are finite; a program needn't handle non-finite values.
Results may differ from a plain program's by a relative error of at most 0.015.
Values may be sent and summed in bfloat16 or wider, within the bound.
A program may use at most 128 MiB of HBM per device.

v0:
```python
import math

import jax
import jax.numpy as jnp
from jax import lax
from jax.sharding import PartitionSpec as P

THETA = 10000.0
EPS = 1e-06
NEGATIVE = -1e30


def rotate(values, positions):
    width = values.shape[-1]
    half = width // 2
    freqs = THETA ** (-2.0 * jnp.arange(half, dtype=jnp.float32) / width)
    angle = positions.astype(jnp.float32)[:, None] * freqs[None, :]
    cosine = jnp.cos(angle)
    sine = jnp.sin(angle)
    if values.ndim == 3:
        cosine = cosine[:, None, :]
        sine = sine[:, None, :]
    first = values[..., :half]
    second = values[..., half:]
    return jnp.concatenate(
        [first * cosine - second * sine, first * sine + second * cosine], axis=-1
    )


def normalize(values, gain):
    return values * lax.rsqrt(jnp.mean(values * values, axis=-1, keepdims=True) + EPS) * gain


def block_keys(weights, latent_rows):
    projected = []
    for key_up, value_up in weights:
        keys = jnp.einsum(
            "kr,rhd->khd", latent_rows, key_up, preferred_element_type=jnp.float32
        ).astype(jnp.bfloat16)
        values = jnp.einsum(
            "kr,rhd->khd", latent_rows, value_up, preferred_element_type=jnp.float32
        ).astype(jnp.bfloat16)
        projected.append((keys, values))
    return projected


def attend(carry, queries, projected, rotated_rows, key_pos, query_pos):
    updated = []
    visible = key_pos[None, :] <= query_pos[:, None]
    for state, query, pair in zip(carry, queries, projected):
        query_nope, query_rot, scale = query
        keys, values = pair
        peak, total, accum = state
        scores = (
            jnp.einsum("qhd,khd->hqk", query_nope, keys, preferred_element_type=jnp.float32)
            + jnp.einsum("qhr,kr->hqk", query_rot, rotated_rows, preferred_element_type=jnp.float32)
        ) * scale
        scores = jnp.where(visible[None], scores, NEGATIVE)
        new_peak = jnp.maximum(peak, jnp.max(scores, axis=-1))
        weights = jnp.where(visible[None], jnp.exp(scores - new_peak[..., None]), 0.0)
        factor = jnp.exp(peak - new_peak)
        total = total * factor + jnp.sum(weights, axis=-1)
        accum = accum * factor[..., None] + jnp.einsum(
            "hqk,khv->hqv", weights.astype(jnp.bfloat16), values, preferred_element_type=jnp.float32
        )
        updated.append((new_peak, total, accum))
    return tuple(updated)


def fold_piece(carry, latent_piece, rotated_piece, piece_pos, weights, segments):
    count = latent_piece.shape[0]
    block = math.gcd(count, 1024)
    last_all = segments[0][1][-1]

    def one_block(index, state):
        lat_rows = lax.dynamic_slice_in_dim(latent_piece, index * block, block, 0)
        rot_rows = lax.dynamic_slice_in_dim(rotated_piece, index * block, block, 0)
        pos_rows = lax.dynamic_slice_in_dim(piece_pos, index * block, block, 0)
        first_key = jnp.min(pos_rows)

        def work(inner):
            projected = block_keys(weights, lat_rows)
            results = []
            for inner_seg, segment in zip(inner, segments):
                queries, seg_pos = segment
                results.append(
                    lax.cond(
                        first_key <= seg_pos[-1],
                        lambda held, queries=queries, seg_pos=seg_pos: attend(
                            held, queries, projected, rot_rows, pos_rows, seg_pos
                        ),
                        lambda held: held,
                        inner_seg,
                    )
                )
            return tuple(results)

        return lax.cond(first_key <= last_all, work, lambda inner: inner, state)

    return lax.fori_loop(0, count // block, one_block, carry)


def shards(
    residual_in,
    query_lean,
    query_broad,
    latent,
    rope_key,
    latent_gain,
    key_up_lean,
    key_up_broad,
    value_up_lean,
    value_up_broad,
    out_lean,
    out_broad,
    attn_gain,
    mlp_gain,
    gate_weight,
    up_weight,
    down_weight,
):
    tokens_here = query_lean.shape[0]
    n_tp = lax.axis_size("tp")
    share = tokens_here // n_tp
    sp_index = lax.axis_index("sp")
    first = sp_index * tokens_here
    query_pos = first + jnp.arange(tokens_here, dtype=jnp.int32)
    rope_width = rope_key.shape[1]
    weights = ((key_up_lean, value_up_lean), (key_up_broad, value_up_broad))
    segment_rows = (query_lean, query_broad, query_pos)
    segments = []
    initial = []
    lean_rows, broad_rows, seg_pos = segment_rows
    queries = []
    states = []
    for query, value_up in ((lean_rows, value_up_lean), (broad_rows, value_up_broad)):
        nope = query.shape[2] - rope_width
        query_rot = rotate(query[:, :, nope:].astype(jnp.float32), seg_pos).astype(jnp.bfloat16)
        queries.append((query[:, :, :nope], query_rot, query.shape[2] ** (-0.5)))
        heads = query.shape[1]
        rows = query.shape[0]
        states.append(
            (
                jnp.full((heads, rows), NEGATIVE, jnp.float32),
                jnp.zeros((heads, rows), jnp.float32),
                jnp.zeros((heads, rows, value_up.shape[2]), jnp.float32),
            )
        )
    segments.append((tuple(queries), seg_pos))
    initial.append(tuple(states))
    segments = tuple(segments)
    initial = tuple(initial)
    sent_latent = normalize(latent.astype(jnp.float32), latent_gain).astype(jnp.bfloat16)
    sent_rot = rotate(rope_key.astype(jnp.float32), query_pos).astype(jnp.bfloat16)
    pieces = (
        lax.all_gather(sent_latent, "sp", axis=0, tiled=True),
        lax.all_gather(sent_rot, "sp", axis=0, tiled=True),
    )
    piece_pos = jnp.arange(pieces[0].shape[0], dtype=jnp.int32)
    folded = fold_piece(initial, pieces[0], pieces[1], piece_pos, weights, segments)
    results = [
        [(accum / total[..., None]).astype(jnp.bfloat16) for peak, total, accum in seg_state]
        for seg_state in folded
    ]
    attended = results[0]
    term = jnp.zeros((share * lax.axis_size("tp"), out_lean.shape[2]), jnp.float32)
    for rows_all, weight in ((attended[0], out_lean), (attended[1], out_broad)):
        rows = rows_all
        term = term + jnp.einsum("hqv,hvd->qd", rows, weight, preferred_element_type=jnp.float32)
    head_sum = lax.psum_scatter(
        term.astype(jnp.bfloat16), "tp", scatter_dimension=0, tiled=True
    ).astype(jnp.float32)
    branch = normalize(head_sum, attn_gain)
    kept = (residual_in.astype(jnp.float32) + branch).astype(jnp.bfloat16)
    normed = normalize(kept.astype(jnp.float32), mlp_gain).astype(jnp.bfloat16)
    whole_normed = lax.all_gather(normed, "tp", axis=0, tiled=True)
    gate_whole, up_whole, down_whole = (
        lax.all_gather(gate_weight, "sp", axis=0, tiled=True),
        lax.all_gather(up_weight, "sp", axis=0, tiled=True),
        lax.all_gather(down_weight, "sp", axis=1, tiled=True),
    )
    gate = jnp.dot(whole_normed, gate_whole, preferred_element_type=jnp.float32)
    up = jnp.dot(whole_normed, up_whole, preferred_element_type=jnp.float32)
    hidden = (jax.nn.silu(gate) * up).astype(jnp.bfloat16)
    rows = hidden
    channel_sum = lax.psum_scatter(
        jnp.dot(rows, down_whole, preferred_element_type=jnp.float32).astype(jnp.bfloat16),
        "tp",
        scatter_dimension=0,
        tiled=True,
    ).astype(jnp.float32)
    return (kept.astype(jnp.float32) + 0.5 * channel_sum).astype(jnp.bfloat16)


def solution(mesh):
    in_specs = (
        P(("sp", "tp"), None),
        P("sp", "tp", None),
        P("sp", "tp", None),
        P("sp", None),
        P("sp", None),
        P(),
        P(None, "tp", None),
        P(None, "tp", None),
        P(None, "tp", None),
        P(None, "tp", None),
        P("tp", None, None),
        P("tp", None, None),
        P(),
        P(),
        P("sp", "tp"),
        P("sp", "tp"),
        P("tp", "sp"),
    )
    out_specs = P(("sp", "tp"), None)
    return jax.shard_map(shards, mesh=mesh, in_specs=in_specs, out_specs=out_specs, check_vma=False)
```

profile of v0, /device:TPU:29, one launch (start us, length us, event | category | flops | bytes accessed | tf_op | source)
XLA Modules:
  0.0 532.7 jit_solution(12831282787911574293)
XLA Ops:
  18.7 32.1 %all_gather.19 = bf16[4096,32]{0,1:T(8,128)(2,1)} all-gather(bf16[256,32]{0,1:T(8,128)(2,1)S(1)} %pad_maximum_fusion.2), channel_id=1, replica_groups=mesh['sp'=16,'tp'=2] {'sp'}, dimensions={0}, use_global_device_ids=true | all-gather | bytes 278528 | tf_op jit(solution)/shard_map/all_gather | solution.py:157
  50.8 19.2 %all-gather.6.cloned.1.call-done = bf16[4096,256]{1,0:T(8,128)(2,1)} async-done(((bf16[256,256]{1,0:T(8,128)(2,1)}), bf16[4096,256]{1,0:T(8,128)(2,1)}) %all-gather.6.cloned.1.call-update) | async-done | bytes 2097168 | tf_op jit(solution)/shard_map/all_gather | solution.py:156
  72.7 113.8 %while.24 = (s32[]{:T(128)}, f32[4,256]{1,0:T(4,128)S(1)}, f32[4,256]{1,0:T(4,128)S(1)}, f32[4,256,64]{1,2,0:T(8,128)}, f32[4,256]{1,0:T(4,128)S(1)}, /*index=5*...) while((s32[]{:T(128)}, f32[4,256]{1,0:T(4,128)S(1)}, ...), condition=%wide.region_11.12_spmd.clone, body=%wide.region_1.11_spmd.clone.sunk | while | flops 1768035584 | bytes 76572688 | solution.py:100
  75.9 25.2 %conditional.4 = ((f32[4,256]{1,0:T(4,128)S(1)}, f32[4,256]{1,0:T(4,128)S(1)}, f32[4,256,64]{1,2,0:T(8,128)}, f32[4,256]{1,0:T(4,128)S(1)}, f32[4,256]{1,0:T(4,128)}, /*index=5*/f32[4,256,128]{2,1,0:T(8,128)})) conditional(s32[]{:T(128)} %convert_element_type.184, (f32[4,256]{1,0:T(4,128)S(1)}, f32[4,256]{1,0:T(4,128)S(1)}, f32[4,256,64]{1,2,0:T(8,128)}, ...), branch_computations={%region_3.0_spmd, %region_4.10_spmd} | conditional | flops 1768034560 | bytes 76562976 | solution.py:98
  80.7 2.4 convolution_convert_fusion
  86.1 15.1 %conditional = ((f32[4,256]{1,0:T(4,128)S(1)}, f32[4,256]{1,0:T(4,128)S(1)}, f32[4,256,64]{1,2,0:T(8,128)}, f32[4,256]{1,0:T(4,128)S(1)}, f32[4,256]{1,0:T(4,128)}, /*index=5*/f32[4,256,128]{2,1,0:T(8,128)})) conditional(s32[]{:T(128)} %convert_element_type.80, (f32[4,256]{1,0:T(4,128)S(1)}, f32[4,256]{1,0:T(4,128)S(1)}, f32[4,256,64]{1,2,0:T(8,128)}, ...), branch_computations={%region_5.0_spmd, %region_6.9_spmd} | conditional | flops 961155072 | bytes 57939176 | solution.py:87
  95.7 2.9 fusion.20
  98.6 2.6 fusion.23
  104.4 25.2 %conditional.4 = ((f32[4,256]{1,0:T(4,128)S(1)}, f32[4,256]{1,0:T(4,128)S(1)}, f32[4,256,64]{1,2,0:T(8,128)}, f32[4,256]{1,0:T(4,128)S(1)}, f32[4,256]{1,0:T(4,128)}, /*index=5*/f32[4,256,128]{2,1,0:T(8,128)})) conditional(s32[]{:T(128)} %convert_element_type.184, (f32[4,256]{1,0:T(4,128)S(1)}, f32[4,256]{1,0:T(4,128)S(1)}, f32[4,256,64]{1,2,0:T(8,128)}, ...), branch_computations={%region_3.0_spmd, %region_4.10_spmd} | conditional | flops 1768034560 | bytes 76562976 | solution.py:98
  109.1 2.4 convolution_convert_fusion
  114.5 15.1 %conditional = ((f32[4,256]{1,0:T(4,128)S(1)}, f32[4,256]{1,0:T(4,128)S(1)}, f32[4,256,64]{1,2,0:T(8,128)}, f32[4,256]{1,0:T(4,128)S(1)}, f32[4,256]{1,0:T(4,128)}, /*index=5*/f32[4,256,128]{2,1,0:T(8,128)})) conditional(s32[]{:T(128)} %convert_element_type.80, (f32[4,256]{1,0:T(4,128)S(1)}, f32[4,256]{1,0:T(4,128)S(1)}, f32[4,256,64]{1,2,0:T(8,128)}, ...), branch_computations={%region_5.0_spmd, %region_6.9_spmd} | conditional | flops 961155072 | bytes 57939176 | solution.py:87
  124.1 2.9 fusion.20
  127.0 2.6 fusion.23
  132.8 25.2 %conditional.4 = ((f32[4,256]{1,0:T(4,128)S(1)}, f32[4,256]{1,0:T(4,128)S(1)}, f32[4,256,64]{1,2,0:T(8,128)}, f32[4,256]{1,0:T(4,128)S(1)}, f32[4,256]{1,0:T(4,128)}, /*index=5*/f32[4,256,128]{2,1,0:T(8,128)})) conditional(s32[]{:T(128)} %convert_element_type.184, (f32[4,256]{1,0:T(4,128)S(1)}, f32[4,256]{1,0:T(4,128)S(1)}, f32[4,256,64]{1,2,0:T(8,128)}, ...), branch_computations={%region_3.0_spmd, %region_4.10_spmd} | conditional | flops 1768034560 | bytes 76562976 | solution.py:98
  137.6 2.4 convolution_convert_fusion
  143.0 15.1 %conditional = ((f32[4,256]{1,0:T(4,128)S(1)}, f32[4,256]{1,0:T(4,128)S(1)}, f32[4,256,64]{1,2,0:T(8,128)}, f32[4,256]{1,0:T(4,128)S(1)}, f32[4,256]{1,0:T(4,128)}, /*index=5*/f32[4,256,128]{2,1,0:T(8,128)})) conditional(s32[]{:T(128)} %convert_element_type.80, (f32[4,256]{1,0:T(4,128)S(1)}, f32[4,256]{1,0:T(4,128)S(1)}, f32[4,256,64]{1,2,0:T(8,128)}, ...), branch_computations={%region_5.0_spmd, %region_6.9_spmd} | conditional | flops 961155072 | bytes 57939176 | solution.py:87
  152.6 2.9 fusion.20
  155.4 2.6 fusion.23
  161.3 25.2 %conditional.4 = ((f32[4,256]{1,0:T(4,128)S(1)}, f32[4,256]{1,0:T(4,128)S(1)}, f32[4,256,64]{1,2,0:T(8,128)}, f32[4,256]{1,0:T(4,128)S(1)}, f32[4,256]{1,0:T(4,128)}, /*index=5*/f32[4,256,128]{2,1,0:T(8,128)})) conditional(s32[]{:T(128)} %convert_element_type.184, (f32[4,256]{1,0:T(4,128)S(1)}, f32[4,256]{1,0:T(4,128)S(1)}, f32[4,256,64]{1,2,0:T(8,128)}, ...), branch_computations={%region_3.0_spmd, %region_4.10_spmd} | conditional | flops 1768034560 | bytes 76562976 | solution.py:98
  166.0 2.4 convolution_convert_fusion
  171.4 15.1 %conditional = ((f32[4,256]{1,0:T(4,128)S(1)}, f32[4,256]{1,0:T(4,128)S(1)}, f32[4,256,64]{1,2,0:T(8,128)}, f32[4,256]{1,0:T(4,128)S(1)}, f32[4,256]{1,0:T(4,128)}, /*index=5*/f32[4,256,128]{2,1,0:T(8,128)})) conditional(s32[]{:T(128)} %convert_element_type.80, (f32[4,256]{1,0:T(4,128)S(1)}, f32[4,256]{1,0:T(4,128)S(1)}, f32[4,256,64]{1,2,0:T(8,128)}, ...), branch_computations={%region_5.0_spmd, %region_6.9_spmd} | conditional | flops 961155072 | bytes 57939176 | solution.py:87
  181.0 2.9 fusion.20
  183.9 2.6 fusion.23
  188.5 2.5 fusion.48
  191.0 10.4 %reduce-scatter.3.cloned.1.call-done = bf16[128,2048]{1,0:T(8,128)(2,1)} async-done(((bf16[256,2048]{1,0:T(8,128)(2,1)}), bf16[128,2048]{1,0:T(8,128)(2,1)}) %reduce-scatter.3.cloned.1.call-update) | async-done | bytes 524304 | tf_op jit(solution)/shard_map/reduce_scatter | solution.py:170
  207.1 8.4 %all-gather.8.cloned.1.call-done = bf16[256,2048]{1,0:T(8,128)(2,1)} async-done(((bf16[128,2048]{1,0:T(8,128)(2,1)}), bf16[256,2048]{1,0:T(8,128)(2,1)}) %all-gather.8.cloned.1.call-update) | async-done | bytes 1048592 | tf_op jit(solution)/shard_map/all_gather | solution.py:176
  215.6 90.3 %all-gather.10.cloned.1.call-done = bf16[2048,1408]{1,0:T(8,128)(2,1)} async-done(((bf16[128,1408]{1,0:T(8,128)(2,1)}), bf16[2048,1408]{1,0:T(8,128)(2,1)}) %all-gather.10.cloned.1.call-update) | async-done | bytes 5767184 | tf_op jit(solution)/shard_map/all_gather | solution.py:178
  305.9 5.9 %fusion.70 = f32[256,1408]{1,0:T(8,128)} fusion(bf16[256,2048]{1,0:T(8,128)(2,1)} %all-gather.8.cloned.1.call-done, bf16[2048,1408]{1,0:T(8,128)(2,1)} %all-gather.10.cloned.1.call-done), kind=kOutput, calls=%fused_computation.105 | convolution fusion | flops 1476395008 | bytes 8257536 | tf_op jit(solution)/shard_map/dot_general | solution.py:182
  311.8 84.1 %all-gather.12.cloned.1.call-done = bf16[2048,1408]{1,0:T(8,128)(2,1)} async-done(((bf16[128,1408]{1,0:T(8,128)(2,1)}), bf16[2048,1408]{1,0:T(8,128)(2,1)}) %all-gather.12.cloned.1.call-update) | async-done | bytes 5767184 | tf_op jit(solution)/shard_map/all_gather | solution.py:179
  395.9 109.2 %all-gather.14.cloned.1.call-done = bf16[1408,2048]{1,0:T(8,128)(2,1)} async-done(((bf16[1408,128]{1,0:T(8,128)(2,1)}), bf16[1408,2048]{1,0:T(8,128)(2,1)}) %all-gather.14.cloned.1.call-update) | async-done | bytes 5767184 | tf_op jit(solution)/shard_map/all_gather | solution.py:180
  505.1 9.5 %convolution_convert_fusion.2 = bf16[256,2048]{1,0:T(8,128)(2,1)} fusion(bf16[1408,2048]{1,0:T(8,128)(2,1)} %all-gather.14.cloned.1.call-done, bf16[256,2048]{1,0:T(8,128)(2,1)} %all-gather.8.cloned.1.call-done, bf16[2048,1408]{1,0:T(8,128)(2,1)} %all-gather.12.cloned.1.call-done, f32[256,1408]{1,0:T(8,128)} %fusion.70), kind=kOutput, calls=%fused_computation.57 | convolution fusion | flops 2955476992 | bytes 15073280 | tf_op jit(solution)/shard_map/dot_general | solution.py:187
  514.6 9.3 %reduce-scatter.5.cloned.1.call-done = bf16[128,2048]{1,0:T(8,128)(2,1)} async-done(((bf16[256,2048]{1,0:T(8,128)(2,1)}), bf16[128,2048]{1,0:T(8,128)(2,1)}) %reduce-scatter.5.cloned.1.call-update) | async-done | bytes 524304 | tf_op jit(solution)/shard_map/reduce_scatter | solution.py:186
  (208 shorter events, 95.7 us)
Async XLA Ops:
  6.5 180.0 %copy-start = (bf16[4,128,2048]{2,1,0:T(8,128)(2,1)S(1)}, bf16[4,128,2048]{2,1,0:T(8,128)(2,1)}, u32[]{:S(2)}) copy-start(bf16[4,128,2048]{2,1,0:T(8,128)(2,1)} %param.34) | copy-start | bytes 6291460
  6.5 63.5 %all-gather.6.cloned.1.call-start = ((), (), s32[]{:S(2)}) async-start(), calls=%async_computation.2 | async-start | bytes 2228224 | tf_op jit(solution)/shard_map/all_gather | solution.py:156
  9.4 192.0 %reduce-scatter.3.cloned.1.call-start = ((), (), s32[]{:S(2)}) async-start(), calls=%async_computation.3 | async-start | bytes 1572864 | tf_op jit(solution)/shard_map/reduce_scatter | solution.py:170
  76.0 4.7 copy-start.1
  77.5 6.0 %copy-start.11 = (s32[256]{0:T(256)S(1)}, s32[256]{0:T(256)}, u32[]{:S(2)}) copy-start(s32[256]{0:T(256)} %get-tuple-element.684) | copy-start | bytes 3076 | tf_op jit(solution)/shard_map/while/body/eval_jaxpr/cond
  86.1 2.7 copy-start.5
  86.1 2.7 copy-start.6
  92.3 3.4 copy-start.2
  94.3 4.2 copy-start.3
  104.4 4.7 copy-start.1
  106.0 6.0 %copy-start.11 = (s32[256]{0:T(256)S(1)}, s32[256]{0:T(256)}, u32[]{:S(2)}) copy-start(s32[256]{0:T(256)} %get-tuple-element.684) | copy-start | bytes 3076 | tf_op jit(solution)/shard_map/while/body/eval_jaxpr/cond
  114.5 2.7 copy-start.5
  120.7 3.4 copy-start.2
  122.8 4.2 copy-start.3
  132.8 4.7 copy-start.1
  134.4 6.0 %copy-start.11 = (s32[256]{0:T(256)S(1)}, s32[256]{0:T(256)}, u32[]{:S(2)}) copy-start(s32[256]{0:T(256)} %get-tuple-element.684) | copy-start | bytes 3076 | tf_op jit(solution)/shard_map/while/body/eval_jaxpr/cond
  149.1 3.4 copy-start.2
  151.2 4.2 copy-start.3
  161.3 4.7 copy-start.1
  162.9 6.0 %copy-start.11 = (s32[256]{0:T(256)S(1)}, s32[256]{0:T(256)}, u32[]{:S(2)}) copy-start(s32[256]{0:T(256)} %get-tuple-element.684) | copy-start | bytes 3076 | tf_op jit(solution)/shard_map/while/body/eval_jaxpr/cond
  171.4 2.7 copy-start.5
  171.4 2.7 copy-start.6
  177.6 3.4 copy-start.2
  179.7 4.2 copy-start.3
  188.4 14.2 %copy-start.9 = (bf16[128,2048]{1,0:T(8,128)(2,1)S(1)}, bf16[128,2048]{1,0:T(8,128)(2,1)}, u32[]{:S(2)}) copy-start(bf16[128,2048]{1,0:T(8,128)(2,1)} %param.23) | copy-start | bytes 1572868
  188.4 14.2 %copy-start.12 = (f32[2048]{0:T(1024)S(1)}, f32[2048]{0:T(1024)}, u32[]{:S(2)}) copy-start(f32[2048]{0:T(1024)} %param.35) | copy-start | bytes 24580
  188.5 15.7 %copy-start.13 = (f32[2048]{0:T(1024)S(1)}, f32[2048]{0:T(1024)}, u32[]{:S(2)}) copy-start(f32[2048]{0:T(1024)} %param.36) | copy-start | bytes 24580
  191.0 24.6 %all-gather.8.cloned.1.call-start = ((), (), s32[]{:S(2)}) async-start(), calls=%async_computation.4 | async-start | bytes 1572864 | tf_op jit(solution)/shard_map/all_gather | solution.py:176
  205.2 100.7 %all-gather.10.cloned.1.call-start = ((), (), s32[]{:S(2)}) async-start(), calls=%async_computation.5 | async-start | bytes 6127616 | tf_op jit(solution)/shard_map/all_gather | solution.py:178
  205.7 190.1 %all-gather.12.cloned.1.call-start = ((), (), s32[]{:S(2)}) async-start(), calls=%async_computation.6 | async-start | bytes 6127616 | tf_op jit(solution)/shard_map/all_gather | solution.py:179
  206.3 298.8 %all-gather.14.cloned.1.call-start = ((), (), s32[]{:S(2)}) async-start(), calls=%async_computation.7 | async-start | bytes 6127616 | tf_op jit(solution)/shard_map/all_gather | solution.py:180
  206.9 317.0 %reduce-scatter.5.cloned.1.call-start = ((), (), s32[]{:S(2)}) async-start(), calls=%async_computation.8 | async-start | bytes 1572864 | tf_op jit(solution)/shard_map/reduce_scatter | solution.py:186
  (16 other events, 21.2 us)
Sparse Core Ops, SparseCore 0:
  10.1 59.8 all-gather.5
  191.1 10.2 reduce-scatter.2
  205.3 10.2 all-gather.7
  218.1 87.7 all-gather.9
  308.4 87.4 all-gather.11
  398.4 106.6 all-gather.13
  514.7 9.1 reduce-scatter.4
where the time goes:
time: 536 us; the launch traced here: 533 us
  waiting for transfers between devices  333 us (62%)
  matrix products  84.8 us (16%)
  other arithmetic  41.5 us (8%)
  blocking collectives  32.1 us (6%)
  local copies, waits for them, and re-layouts  16.7 us (3%)
  between operations  13.6 us (3%)
  loops' own time  11.1 us (2%)
    all_gather x1, waiting for transfers between devices, shards(): lax.all_gather(down_weight, 'sp', axis=1, tiled=True)  109 us
    all_gather x1, waiting for transfers between devices, shards(): lax.all_gather(gate_weight, 'sp', axis=0, tiled=True)  90.3 us
    all_gather x1, waiting for transfers between devices, shards(): lax.all_gather(up_weight, 'sp', axis=0, tiled=True)  84.1 us
    all_gather x1, blocking collectives, shards(): lax.all_gather(sent_rot, 'sp', axis=0, tiled=True)  32.1 us
    dot_general x8, matrix products, attend(): jnp.einsum('hqk,khv->hqv', weights.astype(jnp.bfloat16), values, preferre...  21.9 us
    all_gather x1, waiting for transfers between devices, shards(): lax.all_gather(sent_latent, 'sp', axis=0, tiled=True)  19.2 us
    cond x8, matrix products  11.7 us
  transfers between devices with their start and end apart: 7, of which 7 were waited for; matrix products, arithmetic and copies ran while one was open for 3% of the time, Pallas kernels for 0%

commit v1 on v0

--- a/solution.py
+++ b/solution.py
@@ -1,8 +1,11 @@
+import functools
 import math
 
 import jax
 import jax.numpy as jnp
 from jax import lax
+from jax.experimental import pallas as pl
+from jax.experimental.pallas import tpu as pltpu
 from jax.sharding import PartitionSpec as P
 
 THETA = 10000.0
@@ -192,6 +195,468 @@
     return (kept.astype(jnp.float32) + 0.5 * channel_sum).astype(jnp.bfloat16)
 
 
+LOG2E = math.log2(math.e)
+
+
+def grid_of(mesh):
+    n_sp, n_tp = mesh.shape["sp"], mesh.shape["tp"]
+    devices = mesh.devices.reshape(n_sp, n_tp)
+    try:
+        places = [tuple(device.coords) for device in devices[:, 0]]
+        partners = [tuple(device.coords) for device in devices[:, -1]]
+    except Exception:
+        return (n_sp // 4, 2, 2) if n_sp % 4 == 0 else None
+    if places != partners:
+        return None
+    low = [min(place[k] for place in places) for k in range(3)]
+    sizes = [max(place[k] for place in places) - low[k] + 1 for k in range(3)]
+    wide_z, wide_y, wide_x = sizes[2], sizes[1], sizes[0]
+    if wide_z * wide_y * wide_x != n_sp:
+        return None
+    for index, place in enumerate(places):
+        x, y, z = (place[k] - low[k] for k in range(3))
+        if (z * wide_y + y) * wide_x + x != index:
+            return None
+    return wide_z, wide_y, wide_x
+
+
+def hop_table(grid):
+    wide_z = grid[0]
+    entries = [
+        (dz, fy, fx)
+        for dz in range(1 - wide_z, wide_z)
+        for fy in range(2)
+        for fx in range(2)
+        if (dz, fy, fx) != (0, 0, 0)
+    ]
+    entries.sort(key=lambda e: (abs(e[0]) + e[1] + e[2], abs(e[0]), e))
+    return entries
+
+
+def layer_kernel(
+    grid, shapes, res, ql, qb, lat, lrow, ag, mg, kul, kub, vu, wol, wob, gw, uw, dw, out,
+    lat_all, gate_all, up_all, down_all, ktl, ktb, vals, peak, total, acc, att, term, inbox, kept,
+    normed, hidden, inbox2, lat_recv, lat_send, lat_pair, recv, send, own_sem, pair_send, pair_recv,
+):
+    wide_z, wide_y, wide_x = grid
+    n_sp = wide_z * wide_y * wide_x
+    tokens, share, rope = shapes
+    heads_l, heads_b = ql.shape[0], qb.shape[0]
+    bf16, f32 = jnp.bfloat16, jnp.float32
+    me = lax.axis_index("sp")
+    core = lax.axis_index("tp")
+    my_x = lax.rem(me, wide_x)
+    my_y = lax.rem(me // wide_x, wide_y)
+    my_z = me // (wide_x * wide_y)
+    here = (my_z, my_y, my_x)
+    strides = (wide_y * wide_x, wide_x, 1)
+    Z, Y, X = 0, 1, 2
+    flip_y = me + (1 - 2 * my_y) * strides[1]
+    flip_x = me + (1 - 2 * my_x)
+    ways = (
+        (X, None, None, flip_x),
+        (Y, None, None, flip_y),
+        (Z, -1, my_z > 0, jnp.maximum(me - strides[0], 0)),
+        (Z, 1, my_z < wide_z - 1, jnp.minimum(me + strides[0], n_sp - 1)),
+    )
+
+    barrier = pltpu.get_barrier_semaphore()
+    for dim, sign, exists, where in ways:
+        def greet(where=where):
+            pl.semaphore_signal(barrier, inc=1, device_id={"sp": where})
+        if exists is None:
+            greet()
+        else:
+            pl.when(exists)(greet)
+    pl.semaphore_signal(barrier, inc=1, device_id={"tp": 1 - core})
+    ends = jnp.where(my_z > 0, 1, 0) + jnp.where(my_z < wide_z - 1, 1, 0)
+    pl.semaphore_wait(barrier, 3 + ends)
+
+    def wanted(order, origin, way):
+        dim, sign, exists, _ = way
+        place = order.index(dim)
+        ok = origin[dim] == here[dim] if sign is None else sign * (here[dim] - origin[dim]) >= 0
+        for later in order[place + 1:]:
+            ok = jnp.logical_and(ok, origin[later] == here[later])
+        return ok if exists is None else jnp.logical_and(ok, exists)
+
+    def index_of(origin):
+        return origin[0] * strides[0] + origin[1] * strides[1] + origin[2]
+
+    gate_rows, units = gw.shape
+    down_cols = dw.shape[1]
+    cut = units // 4
+    ORDER_A, ORDER_B, ORDER_C, ORDER_D = (Z, X, Y), (Z, Y, X), (X, Y, Z), (Y, X, Z)
+
+    def gate_at(ref):
+        return lambda i: ref.at[pl.ds(pl.multiple_of(i * gate_rows, gate_rows), gate_rows)]
+
+    def down_at(k):
+        return lambda i: down_all.at[
+            pl.ds(k * cut, cut), pl.ds(pl.multiple_of(i * down_cols, down_cols), down_cols)
+        ]
+
+    parts = [
+        (ORDER_A, gw, gate_at(gate_all)),
+        (ORDER_B, uw, gate_at(up_all)),
+    ] + [
+        (order, dw.at[pl.ds(k * cut, cut)], down_at(k))
+        for k, order in enumerate((ORDER_A, ORDER_B, ORDER_C, ORDER_D))
+    ]
+
+    def part_copy(p, w, i, mine):
+        order, own, at = parts[p]
+        return pltpu.make_async_remote_copy(
+            src_ref=own if mine else at(i), dst_ref=at(i), send_sem=send.at[p, w, i],
+            recv_sem=recv.at[p, i], device_id={"sp": ways[w][3]},
+        )
+
+    half = lat.shape[0] // 2
+    first = pl.multiple_of(core * half, half)
+
+    def lat_at(i):
+        return lat_all.at[i, pl.ds(first, half)]
+
+    def lat_copy(w, i, mine):
+        return pltpu.make_async_remote_copy(
+            src_ref=lat.at[pl.ds(first, half)] if mine else lat_at(i), dst_ref=lat_at(i),
+            send_sem=lat_send.at[w, i], recv_sem=lat_recv.at[i], device_id={"sp": ways[w][3]},
+        )
+
+    def pair_lat(i):
+        return pltpu.make_async_remote_copy(
+            src_ref=lat_at(i), dst_ref=lat_at(i), send_sem=lat_pair.at[0, i],
+            recv_sem=lat_pair.at[1, i], device_id={"tp": 1 - core},
+        )
+
+    def run(condition, action):
+        if condition is None:
+            action()
+        else:
+            pl.when(condition)(action)
+
+    for w, way in enumerate(ways):
+        run(way[2], lambda w=w: lat_copy(w, me, True).start())
+    own = [pltpu.make_async_copy(lat, lat_all.at[me], own_sem.at[0])]
+    for p, (_, src, at) in enumerate(parts):
+        own.append(pltpu.make_async_copy(src, at(me), own_sem.at[1 + p]))
+    for copy in own:
+        copy.start()
+
+    def send_own(w):
+        for p in range(len(parts)):
+            run(ways[w][2], lambda p=p: part_copy(p, w, me, True).start())
+
+    send_own(0)
+
+    table = hop_table(grid)
+    codes = [((dz + wide_z - 1) * 2 + fy) * 2 + fx for dz, fy, fx in table]
+    per = 4
+    words = [
+        sum(code << (7 * k) for k, code in enumerate(codes[at:at + per]))
+        for at in range(0, len(codes), per)
+    ]
+
+    def origin_of(n):
+        word = jnp.int32(words[0])
+        for k in range(1, len(words)):
+            word = jnp.where(n // per == k, jnp.int32(words[k]), word)
+        rem = lax.rem(n, per)
+        for k in range(1, per):
+            word = jnp.where(rem >= k, word // 128, word)
+        code = lax.rem(word, 128)
+        dz = code // 4 - (wide_z - 1)
+        fy = lax.rem(code // 2, 2)
+        fx = lax.rem(code, 2)
+        oz = my_z + dz
+        oy = my_y + fy * (1 - 2 * my_y)
+        ox = my_x + fx * (1 - 2 * my_x)
+        return (oz, oy, ox), jnp.logical_and(oz >= 0, oz < wide_z)
+
+    def lat_event(n, _):
+        origin, valid = origin_of(n)
+
+        @pl.when(valid)
+        def _():
+            i = index_of(origin)
+            lat_copy(0, i, False).wait_recv()
+            for w, way in enumerate(ways):
+                run(wanted(ORDER_C, origin, way), lambda w=w: lat_copy(w, i, False).start())
+            pair_lat(i).start()
+
+        return 0
+
+    def part_event(n, _):
+        origin, valid = origin_of(n)
+
+        @pl.when(valid)
+        def _():
+            i = index_of(origin)
+            for p, (order, _, _) in enumerate(parts):
+                part_copy(p, 0, i, False).wait_recv()
+                for w, way in enumerate(ways):
+                    run(wanted(order, origin, way), lambda p=p, w=w: part_copy(p, w, i, False).start())
+
+        return 0
+
+    count = len(table)
+    early = sum(1 for dz, fy, fx in table if abs(dz) + fy + fx <= 2)
+    lax.fori_loop(0, early, lat_event, 0)
+    send_own(1)
+    lax.fori_loop(early, count, lat_event, 0)
+    send_own(2)
+    send_own(3)
+    for copy in own:
+        copy.wait()
+
+    def lat_arrived(i, _):
+        pl.when(i != me)(lambda: pair_lat(i).wait_recv())
+        return 0
+
+    lax.fori_loop(0, n_sp, lat_arrived, 0)
+
+    peak[...] = jnp.full(peak.shape, NEGATIVE, f32)
+    total[...] = jnp.zeros(total.shape, f32)
+    acc[...] = jnp.zeros(acc.shape, f32)
+    wide_l = kul.shape[0] // heads_l
+    wide_b = kub.shape[0] // heads_b
+    lanes = 2 * wide_l
+    contract = (((1,), (1,)), ((), ()))
+
+    def attend_block(j):
+        rows = lat_all[j, :tokens, :]
+        rot = lat_all[j, tokens:, :]
+        for ups, keys, heads, wide in ((kul, ktl, heads_l, wide_l), (kub, ktb, heads_b, wide_b)):
+            made = lax.dot_general(ups[...], rows, contract, preferred_element_type=f32).astype(bf16)
+            for h in range(heads):
+                keys[h, :wide, :] = made[h * wide:(h + 1) * wide]
+                keys[h, wide:, :] = rot
+        vals[...] = jnp.dot(rows, vu[...], preferred_element_type=f32).astype(bf16)
+        row_pos = lax.broadcasted_iota(jnp.int32, (tokens, tokens), 0) + (me - j) * tokens
+        visible = lax.broadcasted_iota(jnp.int32, (tokens, tokens), 1) <= row_pos
+        for g in range(heads_l + heads_b):
+            if g < heads_l:
+                query, keys, col = ql[g], ktl[g], (g // 2) * lanes
+            else:
+                query, keys = qb[g - heads_l], ktb[g - heads_l]
+                col = heads_l * wide_l + (g - heads_l) * wide_b
+            scores = jnp.dot(query, keys, preferred_element_type=f32) * (
+                LOG2E * query.shape[1] ** (-0.5)
+            )
+            scores = jnp.where(visible, scores, NEGATIVE)
+            old = peak[g]
+            new = jnp.maximum(old, jnp.max(scores, axis=-1, keepdims=True))
+            weights = jnp.exp2(scores - new)
+            factor = jnp.exp2(old - new)
+            peak[g] = new
+            total[g] = total[g] * factor + jnp.sum(weights, axis=-1, keepdims=True)
+            acc[g] = acc[g] * factor + jnp.dot(
+                weights.astype(bf16), vals[:, col:col + wide_b], preferred_element_type=f32
+            )
+
+    def step(j, _):
+        lax.fori_loop((j * early) // n_sp, ((j + 1) * early) // n_sp, part_event, 0)
+        pl.when(j <= me)(lambda: attend_block(j))
+        return 0
+
+    lax.fori_loop(0, n_sp, step, 0)
+
+    low = lax.broadcasted_iota(jnp.int32, (tokens, lanes), 1) < wide_l
+    for pair in range(heads_l // 2):
+        both = [acc[2 * pair + k] / total[2 * pair + k] for k in range(2)]
+        att[:, pair * lanes:(pair + 1) * lanes] = jnp.where(low, both[0], both[1]).astype(bf16)
+    split = heads_l * wide_l
+    for h in range(heads_b):
+        g = heads_l + h
+        att[:, split + h * wide_b:split + (h + 1) * wide_b] = (acc[g] / total[g]).astype(bf16)
+
+    features = out.shape[1]
+    block = math.gcd(features, 512)
+
+    def project(n, _):
+        cols = pl.ds(pl.multiple_of(n * block, block), block)
+        term[:, cols] = (
+            jnp.dot(att[:, :split], wol[:, cols], preferred_element_type=f32)
+            + jnp.dot(att[:, split:], wob[:, cols], preferred_element_type=f32)
+        ).astype(bf16)
+        return 0
+
+    lax.fori_loop(0, features // block, project, 0)
+    mine = pl.ds(pl.multiple_of(core * share, share), share)
+    theirs = pl.ds(pl.multiple_of((1 - core) * share, share), share)
+
+    def to_pair(k, src, dst):
+        return pltpu.make_async_remote_copy(
+            src_ref=src, dst_ref=dst, send_sem=pair_send.at[k], recv_sem=pair_recv.at[k],
+            device_id={"tp": 1 - core},
+        )
+
+    heads_out = to_pair(0, term.at[theirs], inbox)
+    heads_out.start()
+    heads_out.wait_recv()
+    rows_at_once = math.gcd(share, 16)
+
+    def norms(n, _):
+        rows = pl.ds(pl.multiple_of(n * rows_at_once, rows_at_once), rows_at_once)
+        full = pl.ds(pl.multiple_of(core * share + n * rows_at_once, rows_at_once), rows_at_once)
+        summed = term[full, :].astype(f32) + inbox[rows, :].astype(f32)
+        branch = normalize(summed, ag[...])
+        mixed = (res[rows, :].astype(f32) + branch).astype(bf16)
+        kept[rows, :] = mixed
+        normed[full, :] = normalize(mixed.astype(f32), mg[...]).astype(bf16)
+        return 0
+
+    lax.fori_loop(0, share // rows_at_once, norms, 0)
+    rows_out = to_pair(1, normed.at[mine], normed.at[mine])
+    rows_out.start()
+    lax.fori_loop(early, count, part_event, 0)
+    to_pair(1, normed.at[theirs], normed.at[theirs]).wait_recv()
+
+    def feed(cols):
+        gate = jnp.dot(normed[...], gate_all[:, cols], preferred_element_type=f32)
+        up = jnp.dot(normed[...], up_all[:, cols], preferred_element_type=f32)
+        hidden[:, cols] = (gate / (1.0 + jnp.exp(-gate)) * up).astype(bf16)
+
+    span = 256
+
+    def feed_loop(n, _):
+        feed(pl.ds(pl.multiple_of(n * span, span), span))
+        return 0
+
+    lax.fori_loop(0, units // span, feed_loop, 0)
+    if units % span:
+        feed(pl.ds(units // span * span, units % span))
+    heads_out.wait_send()
+    wide_n = math.gcd(features, 256)
+
+    def down(n, _):
+        cols = pl.ds(pl.multiple_of(n * wide_n, wide_n), wide_n)
+        term[:, cols] = jnp.dot(
+            hidden[...], down_all[:, cols], preferred_element_type=f32
+        ).astype(bf16)
+        return 0
+
+    lax.fori_loop(0, features // wide_n, down, 0)
+    sums_out = to_pair(2, term.at[theirs], inbox2)
+    sums_out.start()
+
+    def sent(i, _):
+        origin = (i // strides[0], lax.rem(i // strides[1], wide_y), lax.rem(i, wide_x))
+        for w, way in enumerate(ways):
+            run(wanted(ORDER_C, origin, way), lambda w=w: lat_copy(w, i, False).wait_send())
+            for p, (order, _, _) in enumerate(parts):
+                run(wanted(order, origin, way), lambda p=p, w=w: part_copy(p, w, i, False).wait_send())
+        pl.when(i != me)(lambda: pair_lat(i).wait_send())
+        return 0
+
+    lax.fori_loop(0, n_sp, sent, 0)
+    rows_out.wait_send()
+    sums_out.wait_recv()
+
+    def finish(n, _):
+        rows = pl.ds(pl.multiple_of(n * rows_at_once, rows_at_once), rows_at_once)
+        full = pl.ds(pl.multiple_of(core * share + n * rows_at_once, rows_at_once), rows_at_once)
+        summed = term[full, :].astype(f32) + inbox2[rows, :].astype(f32)
+        out[rows, :] = (kept[rows, :].astype(f32) + 0.5 * summed).astype(bf16)
+        return 0
+
+    lax.fori_loop(0, share // rows_at_once, finish, 0)
+    sums_out.wait_send()
+
+
+def fused_shards(
+    grid, residual_in, query_lean, query_broad, latent, rope_key, latent_gain, key_up_lean,
+    key_up_broad, value_up_lean, value_up_broad, out_lean, out_broad, attn_gain, mlp_gain,
+    gate_weight, up_weight, down_weight,
+):
+    bf16, f32 = jnp.bfloat16, jnp.float32
+    tokens = query_lean.shape[0]
+    share, features = residual_in.shape
+    rank = latent.shape[1]
+    rope = rope_key.shape[1]
+    n_sp = lax.axis_size("sp")
+    positions = lax.axis_index("sp") * tokens + jnp.arange(tokens, dtype=jnp.int32)
+
+    def turned(query):
+        nope = query.shape[2] - rope
+        rot = rotate(query[:, :, nope:].astype(f32), positions).astype(bf16)
+        return jnp.transpose(jnp.concatenate([query[:, :, :nope], rot], axis=-1), (1, 0, 2))
+
+    ql, qb = turned(query_lean), turned(query_broad)
+    lat = normalize(latent.astype(f32), latent_gain).astype(bf16)
+    rot_key = rotate(rope_key.astype(f32), positions).astype(bf16)
+    lat = jnp.concatenate([lat, rot_key.T], axis=0)
+    kul = key_up_lean.reshape(rank, -1).T
+    kub = key_up_broad.reshape(rank, -1).T
+    vu = jnp.concatenate([value_up_lean.reshape(rank, -1), value_up_broad.reshape(rank, -1)], axis=1)
+    wol = out_lean.reshape(-1, features)
+    wob = out_broad.reshape(-1, features)
+    heads = ql.shape[0] + qb.shape[0]
+    units = gate_weight.shape[1]
+    wide_b = value_up_broad.shape[2]
+    vmem = pl.BlockSpec(memory_space=pltpu.VMEM)
+    args = (
+        residual_in, ql, qb, lat, lat[:1], attn_gain[None], mlp_gain[None], kul, kub, vu, wol, wob,
+        gate_weight, up_weight, down_weight,
+    )
+    dma = pltpu.SemaphoreType.DMA
+    return pl.pallas_call(
+        functools.partial(layer_kernel, grid, (tokens, share, rope)),
+        out_shape=jax.ShapeDtypeStruct((share, features), bf16),
+        in_specs=[vmem] * len(args),
+        out_specs=vmem,
+        scratch_shapes=[
+            pltpu.VMEM((n_sp, tokens + rope, rank), bf16),
+            pltpu.VMEM((features, units), bf16),
+            pltpu.VMEM((features, units), bf16),
+            pltpu.VMEM((units, features), bf16),
+            pltpu.VMEM((ql.shape[0], ql.shape[2], tokens), bf16),
+            pltpu.VMEM((qb.shape[0], qb.shape[2], tokens), bf16),
+            pltpu.VMEM((tokens, vu.shape[1]), bf16),
+            pltpu.VMEM((heads, tokens, 1), f32),
+            pltpu.VMEM((heads, tokens, 1), f32),
+            pltpu.VMEM((heads, tokens, wide_b), f32),
+            pltpu.VMEM((tokens, vu.shape[1]), bf16),
+            pltpu.VMEM((tokens, features), bf16),
+            pltpu.VMEM((share, features), bf16),
+            pltpu.VMEM((share, features), bf16),
+            pltpu.VMEM((tokens, features), bf16),
+            pltpu.VMEM((tokens, units), bf16),
+            pltpu.VMEM((share, features), bf16),
+            dma((n_sp,)),
+            dma((4, n_sp)),
+            dma((2, n_sp)),
+            dma((6, n_sp)),
+            dma((6, 4, n_sp)),
+            dma((7,)),
+            dma((3,)),
+            dma((3,)),
+        ],
+        compiler_params=pltpu.CompilerParams(
+            collective_id=0, has_side_effects=True, vmem_limit_bytes=62 * 2**20
+        ),
+    )(*args)
+
+
+def fits(grid, mesh, args):
+    if grid is None or mesh.shape["tp"] != 2 or grid[1] != 2 or grid[2] != 2 or grid[0] > 8:
+        return False
+    n_sp = mesh.shape["sp"]
+    tokens = args[1].shape[0] // n_sp
+    share = tokens // 2
+    units = args[14].shape[1] // 2
+    heads_l, heads_b = args[6].shape[1] // 2, args[7].shape[1] // 2
+    wide_l, wide_b = args[6].shape[2], args[7].shape[2]
+    rope = args[4].shape[1]
+    return (
+        tokens % 128 == 0 and tokens <= 256 and share % 16 == 0 and units % 128 == 0
+        and units % 64 == 0 and heads_l % 2 == 0 and 2 * wide_l == wide_b and wide_b % 128 == 0
+        and args[3].shape[1] == tokens and rope % 16 == 0 and (tokens + rope) % 32 == 0
+        and heads_b > 0 and args[8].shape[2] == wide_l and args[9].shape[2] == wide_b
+        and (args[14].shape[0] // n_sp) % 16 == 0 and (args[16].shape[1] // n_sp) % 128 == 0
+    )
+
+
 def solution(mesh):
     in_specs = (
         P(("sp", "tp"), None),
@@ -213,4 +678,12 @@
         P("tp", "sp"),
     )
     out_specs = P(("sp", "tp"), None)
-    return jax.shard_map(shards, mesh=mesh, in_specs=in_specs, out_specs=out_specs, check_vma=False)
+    grid = grid_of(mesh)
+
+    def layer(*args):
+        body = functools.partial(fused_shards, grid) if fits(grid, mesh, args) else shards
+        return jax.shard_map(
+            body, mesh=mesh, in_specs=in_specs, out_specs=out_specs, check_vma=False
+        )(*args)
+
+    return layer

time: 536 us -> 192 us (0.36)
  waiting for transfers between devices: 333 us -> 0 us
  Pallas kernels: 0 us -> 180 us
  matrix products: 84.8 us -> 0 us
  other arithmetic: 41.5 us -> 5 us
  blocking collectives: 32.1 us -> 0 us
  between operations: 13.6 us -> 0.16 us
  loops' own time: 11.1 us -> 0 us
  local copies, waits for them, and re-layouts: 16.7 us -> 6.59 us
    all_gather x5 -> x0, waiting for transfers between devices: 311 us -> none  [the longest x1 109 us: shards(): lax.all_gather(down_weight, 'sp', axis=1, tiled=True)]
    pallas_call x0 -> x1, Pallas kernels: none -> 180 us  [fused_shards(): pl.pallas_call(functools.partial(layer_kernel, grid, (tokens, share, rope...]
    dot_general x36 -> x0, matrix products: 73 us -> none  [the longest x8 21.9 us: attend(): jnp.einsum('hqk,khv->hqv', weights.astype(jnp.bfloat16), values, preferre...]
    all_gather x1 -> x0, blocking collectives: 32.1 us -> none  [shards(): lax.all_gather(sent_rot, 'sp', axis=0, tiled=True)]
    reduce_scatter x2 -> x0, waiting for transfers between devices: 19.7 us -> none  [the longest x1 10.4 us: shards(): lax.psum_scatter(term.astype(jnp.bfloat16), 'tp', scatter_dimension=0, ti...]
    convert_element_type x13 -> x5, other arithmetic: 13.2 us -> 0.9 us  [the longest x1 0.72 us: fused_shards(): rot_key = rotate(rope_key.astype(f32), positions).astype(bf16)]
    cond x8 -> x0, matrix products: 11.7 us -> none
    another operation x9 -> x0, loops' own time: 11.1 us -> none  [the longest x4 5.61 us: one_block(): return lax.cond(first_key <= last_all, work, lambda inner: inner, state)]
  transfers between devices with their start and end apart: 7 -> 0, of which waited for: 7 -> 0; matrix products, arithmetic and copies ran while one was open for 3% -> 0% of each run, Pallas kernels for 0% -> 0%
where the time goes in v1:
time: 192 us
  Pallas kernels  180 us (94%)
  local copies, waits for them, and re-layouts  6.59 us (3%)
  other arithmetic  5 us (3%)
    pallas_call x1, Pallas kernels, fused_shards(): pl.pallas_call(functools.partial(layer_kernel, grid, (tokens, share, rope...  180 us

profile of v1, /device:TPU:29, one launch (start us, length us, event | category | flops | bytes accessed | tf_op | source)
XLA Modules:
  0.0 191.8 jit_solution(8698105253062941677)
XLA Ops:
  0.0 0.7 convert_element_type.32
  0.7 0.1 subtract_convert_fusion.2
  0.9 0.1 copy.28
  1.0 0.1 copy.29
  1.1 0.9 slice.34
  1.9 0.2 copy.35
  2.2 0.9 slice.38
  3.0 0.2 copy.37
  3.2 0.0 slice-start
  3.3 0.4 subtract_convert_fusion
  3.7 0.0 slice-start.1
  3.7 0.0 copy-start
  3.7 0.0 copy-start.4
  3.7 0.5 slice-done
  4.2 0.2 copy.36
  4.4 0.0 copy-start.3
  4.4 1.0 maximum_bitcast_fusion.qb
  5.3 0.0 slice-done.1
  5.3 0.2 copy.34
  5.5 1.0 maximum_bitcast_fusion.1.ql
  6.5 0.0 copy-done
  6.5 0.1 fusion
  6.6 0.1 fusion.2
  6.7 0.7 pad_maximum_fusion.1.lat
  7.4 0.6 slice.50.lrow
  8.0 0.0 copy-done.1
  8.1 0.0 copy-done.3
  8.1 0.1 copy.33
  8.2 0.8 pad_maximum_fusion.vu
  9.0 0.9 copy.32
  9.9 180.0 %shard_map.163 = bf16[128,2048]{1,0:T(8,128)(2,1)} custom-call(bf16[128,2048]{1,0:T(8,128)(2,1)} %res.1, bf16[4,256,96]{2,1,0:T(8,128)(2,1)} %maximum_bitcast_fusion.1.ql, bf16[4,256,160]{2,1,0:T(8,128)(2,1)} %maximum_bitcast_fusion.qb, bf16[288,256]{1,0:T(8,128)(2,1)} %pad_maximum_fusion.1.lat, bf16[1,256]{1,0:T(2,128)(2,1)} %slice.50.lrow, ...), custom_call_target="tpu_custom_call" | custom-call | tf_op jit(solution)/shard_map/pallas_call | solution.py:603
  189.9 1.9 copy.42
  (11 shorter events, 0.1 us)
Async XLA Ops:
  3.2 1.0 slice-start
  3.7 1.6 slice-start.1
  3.7 2.8 %copy-start = (bf16[256,256]{1,0:T(8,128)(2,1)S(1)}, bf16[256,256]{1,0:T(8,128)(2,1)}, u32[]{:S(2)}) copy-start(bf16[256,256]{1,0:T(8,128)(2,1)} %param.20) | copy-start | bytes 393220
  3.7 2.9 %copy-start.4 = (f32[256]{0:T(256)S(1)}, f32[256]{0:T(256)}, u32[]{:S(2)}) copy-start(f32[256]{0:T(256)} %param.22) | copy-start | bytes 3076
  4.2 3.8 %copy-start.1 = (bf16[256,4,128]{2,1,0:T(4,128)(2,1)S(1)}, bf16[256,4,128]{2,1,0:T(4,128)(2,1)}, u32[]{:S(2)}) copy-start(bf16[256,4,128]{2,1,0:T(4,128)(2,1)} %param.26) | copy-start | bytes 786436
  4.4 3.7 %copy-start.3 = (bf16[256,4,64]{0,2,1:T(8,128)(2,1)S(1)}, bf16[256,4,64]{0,2,1:T(8,128)(2,1)}, u32[]{:S(2)}) copy-start(bf16[256,4,64]{0,2,1:T(8,128)(2,1)} %param.25) | copy-start | bytes 393220
  5.3 3.6 %copy-start.2 = (bf16[256,4,128]{2,1,0:T(4,128)(2,1)S(1)}, bf16[256,4,128]{2,1,0:T(4,128)(2,1)}, u32[]{:S(2)}) copy-start(bf16[256,4,128]{2,1,0:T(4,128)(2,1)} %param.24) | copy-start | bytes 786436

commit v2 on v1

--- a/solution.py
+++ b/solution.py
@@ -234,14 +234,14 @@
 
 
 def layer_kernel(
-    grid, shapes, res, ql, qb, lat, lrow, ag, mg, kul, kub, vu, wol, wob, gw, uw, dw, out,
-    lat_all, gate_all, up_all, down_all, ktl, ktb, vals, peak, total, acc, att, term, inbox, kept,
+    grid, shapes, res, qlt, qbt, lat, cosine, sine, ag, mg, kul, kub, vul, vub, wol, wob, gw, uw, dw, out,
+    lat_all, gate_all, up_all, down_all, ql, qb, ktl, ktb, valt_l, valt_b, peak, total, acc_l, acc_b, att, term, inbox, kept,
     normed, hidden, inbox2, lat_recv, lat_send, lat_pair, recv, send, own_sem, pair_send, pair_recv,
 ):
     wide_z, wide_y, wide_x = grid
     n_sp = wide_z * wide_y * wide_x
     tokens, share, rope = shapes
-    heads_l, heads_b = ql.shape[0], qb.shape[0]
+    heads_l, heads_b = qlt.shape[0], qbt.shape[0]
     bf16, f32 = jnp.bfloat16, jnp.float32
     me = lax.axis_index("sp")
     core = lax.axis_index("tp")
@@ -406,6 +406,15 @@
     lax.fori_loop(early, count, lat_event, 0)
     send_own(2)
     send_own(3)
+    half_rope = rope // 2
+    for given, query in ((qlt, ql), (qbt, qb)):
+        nope = given.shape[1] - rope
+        for h in range(given.shape[0]):
+            one = given[h, nope:nope + half_rope, :].astype(f32)
+            two = given[h, nope + half_rope:, :].astype(f32)
+            query[h, :nope, :] = given[h, :nope, :]
+            query[h, nope:nope + half_rope, :] = (one * cosine[...] - two * sine[...]).astype(bf16)
+            query[h, nope + half_rope:, :] = (one * sine[...] + two * cosine[...]).astype(bf16)
     for copy in own:
         copy.wait()
 
@@ -417,13 +426,14 @@
 
     peak[...] = jnp.full(peak.shape, NEGATIVE, f32)
     total[...] = jnp.zeros(total.shape, f32)
-    acc[...] = jnp.zeros(acc.shape, f32)
+    acc_l[...] = jnp.zeros(acc_l.shape, f32)
+    acc_b[...] = jnp.zeros(acc_b.shape, f32)
     wide_l = kul.shape[0] // heads_l
     wide_b = kub.shape[0] // heads_b
-    lanes = 2 * wide_l
     contract = (((1,), (1,)), ((), ()))
-
-    def attend_block(j):
+    contract_rows = (((0,), (0,)), ((), ()))
+
+    def attend_block(j, masked):
         rows = lat_all[j, :tokens, :]
         rot = lat_all[j, tokens:, :]
         for ups, keys, heads, wide in ((kul, ktl, heads_l, wide_l), (kub, ktb, heads_b, wide_b)):
@@ -431,44 +441,51 @@
             for h in range(heads):
                 keys[h, :wide, :] = made[h * wide:(h + 1) * wide]
                 keys[h, wide:, :] = rot
-        vals[...] = jnp.dot(rows, vu[...], preferred_element_type=f32).astype(bf16)
-        row_pos = lax.broadcasted_iota(jnp.int32, (tokens, tokens), 0) + (me - j) * tokens
-        visible = lax.broadcasted_iota(jnp.int32, (tokens, tokens), 1) <= row_pos
+        for ups, held in ((vul, valt_l), (vub, valt_b)):
+            held[...] = lax.dot_general(
+                ups[...], rows, contract, preferred_element_type=f32
+            ).astype(bf16)
+        if masked:
+            key_pos = lax.broadcasted_iota(jnp.int32, (tokens, tokens), 0)
+            visible = key_pos <= lax.broadcasted_iota(jnp.int32, (tokens, tokens), 1)
         for g in range(heads_l + heads_b):
             if g < heads_l:
-                query, keys, col = ql[g], ktl[g], (g // 2) * lanes
+                h, query, keys, held, acc, wide = g, ql, ktl, valt_l, acc_l, wide_l
             else:
-                query, keys = qb[g - heads_l], ktb[g - heads_l]
-                col = heads_l * wide_l + (g - heads_l) * wide_b
-            scores = jnp.dot(query, keys, preferred_element_type=f32) * (
-                LOG2E * query.shape[1] ** (-0.5)
-            )
-            scores = jnp.where(visible, scores, NEGATIVE)
+                h, query, keys, held, acc, wide = g - heads_l, qb, ktb, valt_b, acc_b, wide_b
+            scores = lax.dot_general(
+                keys[h], query[h], contract_rows, preferred_element_type=f32
+            ) * (LOG2E * query.shape[1] ** (-0.5))
+            if masked:
+                scores = jnp.where(visible, scores, NEGATIVE)
             old = peak[g]
-            new = jnp.maximum(old, jnp.max(scores, axis=-1, keepdims=True))
+            new = jnp.maximum(old, jnp.max(scores, axis=0, keepdims=True))
             weights = jnp.exp2(scores - new)
             factor = jnp.exp2(old - new)
             peak[g] = new
-            total[g] = total[g] * factor + jnp.sum(weights, axis=-1, keepdims=True)
-            acc[g] = acc[g] * factor + jnp.dot(
-                weights.astype(bf16), vals[:, col:col + wide_b], preferred_element_type=f32
+            total[g] = total[g] * factor + jnp.sum(weights, axis=0, keepdims=True)
+            acc[h] = acc[h] * factor + jnp.dot(
+                held[h * wide:(h + 1) * wide, :], weights.astype(bf16), preferred_element_type=f32
             )
 
     def step(j, _):
         lax.fori_loop((j * early) // n_sp, ((j + 1) * early) // n_sp, part_event, 0)
-        pl.when(j <= me)(lambda: attend_block(j))
+        pl.when(j < me)(lambda: attend_block(j, False))
         return 0
 
     lax.fori_loop(0, n_sp, step, 0)
-
-    low = lax.broadcasted_iota(jnp.int32, (tokens, lanes), 1) < wide_l
-    for pair in range(heads_l // 2):
-        both = [acc[2 * pair + k] / total[2 * pair + k] for k in range(2)]
-        att[:, pair * lanes:(pair + 1) * lanes] = jnp.where(low, both[0], both[1]).astype(bf16)
+    attend_block(me, True)
+
     split = heads_l * wide_l
-    for h in range(heads_b):
-        g = heads_l + h
-        att[:, split + h * wide_b:split + (h + 1) * wide_b] = (acc[g] / total[g]).astype(bf16)
+    for heads, wide, acc, base, col in (
+        (heads_l, wide_l, acc_l, 0, 0), (heads_b, wide_b, acc_b, heads_l, split),
+    ):
+        together = wide_b // wide
+        for h in range(0, heads, together):
+            done = jnp.concatenate(
+                [acc[h + k] / total[base + h + k] for k in range(together)], axis=0
+            )
+            att[:, col + h * wide:col + (h + together) * wide] = done.T.astype(bf16)
 
     features = out.shape[1]
     block = math.gcd(features, 512)
@@ -577,18 +594,16 @@
     n_sp = lax.axis_size("sp")
     positions = lax.axis_index("sp") * tokens + jnp.arange(tokens, dtype=jnp.int32)
 
-    def turned(query):
-        nope = query.shape[2] - rope
-        rot = rotate(query[:, :, nope:].astype(f32), positions).astype(bf16)
-        return jnp.transpose(jnp.concatenate([query[:, :, :nope], rot], axis=-1), (1, 0, 2))
-
-    ql, qb = turned(query_lean), turned(query_broad)
+    ql, qb = (jnp.transpose(query, (1, 2, 0)) for query in (query_lean, query_broad))
+    freqs = THETA ** (-2.0 * jnp.arange(rope // 2, dtype=f32) / rope)
+    angle = freqs[:, None] * positions.astype(f32)[None, :]
     lat = normalize(latent.astype(f32), latent_gain).astype(bf16)
     rot_key = rotate(rope_key.astype(f32), positions).astype(bf16)
     lat = jnp.concatenate([lat, rot_key.T], axis=0)
     kul = key_up_lean.reshape(rank, -1).T
     kub = key_up_broad.reshape(rank, -1).T
-    vu = jnp.concatenate([value_up_lean.reshape(rank, -1), value_up_broad.reshape(rank, -1)], axis=1)
+    vul = value_up_lean.reshape(rank, -1).T
+    vub = value_up_broad.reshape(rank, -1).T
     wol = out_lean.reshape(-1, features)
     wob = out_broad.reshape(-1, features)
     heads = ql.shape[0] + qb.shape[0]
@@ -596,7 +611,8 @@
     wide_b = value_up_broad.shape[2]
     vmem = pl.BlockSpec(memory_space=pltpu.VMEM)
     args = (
-        residual_in, ql, qb, lat, lat[:1], attn_gain[None], mlp_gain[None], kul, kub, vu, wol, wob,
+        residual_in, ql, qb, lat, jnp.cos(angle), jnp.sin(angle), attn_gain[None], mlp_gain[None],
+        kul, kub, vul, vub, wol, wob,
         gate_weight, up_weight, down_weight,
     )
     dma = pltpu.SemaphoreType.DMA
@@ -610,13 +626,17 @@
             pltpu.VMEM((features, units), bf16),
             pltpu.VMEM((features, units), bf16),
             pltpu.VMEM((units, features), bf16),
-            pltpu.VMEM((ql.shape[0], ql.shape[2], tokens), bf16),
-            pltpu.VMEM((qb.shape[0], qb.shape[2], tokens), bf16),
-            pltpu.VMEM((tokens, vu.shape[1]), bf16),
-            pltpu.VMEM((heads, tokens, 1), f32),
-            pltpu.VMEM((heads, tokens, 1), f32),
-            pltpu.VMEM((heads, tokens, wide_b), f32),
-            pltpu.VMEM((tokens, vu.shape[1]), bf16),
+            pltpu.VMEM(ql.shape, bf16),
+            pltpu.VMEM(qb.shape, bf16),
+            pltpu.VMEM(ql.shape, bf16),
+            pltpu.VMEM(qb.shape, bf16),
+            pltpu.VMEM((vul.shape[0], tokens), bf16),
+            pltpu.VMEM((vub.shape[0], tokens), bf16),
+            pltpu.VMEM((heads, 1, tokens), f32),
+            pltpu.VMEM((heads, 1, tokens), f32),
+            pltpu.VMEM((ql.shape[0], value_up_lean.shape[2], tokens), f32),
+            pltpu.VMEM((qb.shape[0], wide_b, tokens), f32),
+            pltpu.VMEM((tokens, vul.shape[0] + vub.shape[0]), bf16),
             pltpu.VMEM((tokens, features), bf16),
             pltpu.VMEM((share, features), bf16),
             pltpu.VMEM((share, features), bf16),
@@ -651,7 +671,7 @@
     return (
         tokens % 128 == 0 and tokens <= 256 and share % 16 == 0 and units % 128 == 0
         and units % 64 == 0 and heads_l % 2 == 0 and 2 * wide_l == wide_b and wide_b % 128 == 0
-        and args[3].shape[1] == tokens and rope % 16 == 0 and (tokens + rope) % 32 == 0
+        and args[3].shape[1] == tokens and rope % 32 == 0 and (tokens + rope) % 32 == 0
         and heads_b > 0 and args[8].shape[2] == wide_l and args[9].shape[2] == wide_b
         and (args[14].shape[0] // n_sp) % 16 == 0 and (args[16].shape[1] // n_sp) % 128 == 0
     )

time: 192 us -> 171 us (0.89)
  Pallas kernels: 180 us -> 161 us
    pallas_call x1, Pallas kernels: 180 us -> 161 us  [fused_shards(): pl.pallas_call(functools.partial(layer_kernel, grid, (tokens, share, rope...]
    slice x7 -> x0, local copies, waits for them, and re-layouts: 2.77 us -> none  [the longest x2 1.7 us: turned(): rot = rotate(query[:, :, nope:].astype(f32), positions).astype(bf16)]
    unnamed x17 -> x3, local copies, waits for them, and re-layouts: 3.53 us -> 5.5 us
    transpose x2 -> x0, other arithmetic: 1.92 us -> none  [turned(): jnp.transpose(jnp.concatenate([query[:, :, :nope], rot], axis=-1), (1, 0,...]
where the time goes in v2:
time: 171 us
  Pallas kernels  161 us (94%)
  local copies, waits for them, and re-layouts  5.5 us (3%)
  other arithmetic  4.35 us (3%)
    pallas_call x1, Pallas kernels, fused_shards(): pl.pallas_call(functools.partial(layer_kernel, grid, (tokens, share, rope...  161 us
    unnamed x3, local copies, waits for them, and re-layouts  5.5 us

profile of v2, /device:TPU:29, one launch (start us, length us, event | category | flops | bytes accessed | tf_op | source)
XLA Modules:
  0.0 170.7 jit_solution(5670585071892687684)
XLA Ops:
  0.0 1.0 fusion
  1.1 0.7 convert_element_type.24
  1.8 0.1 fusion.8
  1.9 0.8 multiply_sine_fusion
  2.7 1.0 fusion.2
  3.7 0.7 pad_maximum_fusion.lat
  4.4 1.8 %copy.18 = bf16[256,4,128]{0,2,1:T(8,128)(2,1)} copy(bf16[256,4,128]{2,1,0:T(4,128)(2,1)} %param.24) | data formatting | bytes 524288 | tf_op args[7]
  6.2 1.8 %copy.19 = bf16[256,4,128]{0,2,1:T(8,128)(2,1)} copy(bf16[256,4,128]{2,1,0:T(4,128)(2,1)} %param.26) | data formatting | bytes 524288 | tf_op args[9]
  8.0 160.8 %shard_map.163 = bf16[128,2048]{1,0:T(8,128)(2,1)} custom-call(bf16[128,2048]{1,0:T(8,128)(2,1)} %res.1, bf16[4,96,256]{2,1,0:T(8,128)(2,1)} %bitcast.25, bf16[4,160,256]{2,1,0:T(8,128)(2,1)} %bitcast.24, bf16[288,256]{1,0:T(8,128)(2,1)} %pad_maximum_fusion.lat, f32[16,256]{1,0:T(8,128)} %get-tuple-element.8.cosine, f32[16,256]{1,0:T(8,128)} %get-tuple-element.7.sine, ...), custom_call_target="tpu_custom_call" | custom-call | tf_op jit(solution)/shard_map/pallas_call | solution.py:619
  168.8 1.9 %copy.21 = bf16[128,2048]{1,0:T(8,128)(2,1)} copy(bf16[128,2048]{1,0:T(8,128)(2,1)} %shard_map.163) | data formatting | bytes 1048576
  (4 shorter events, 0.0 us)

commit v3 on v2

--- a/solution.py
+++ b/solution.py
@@ -234,9 +234,9 @@
 
 
 def layer_kernel(
-    grid, shapes, res, qlt, qbt, lat, cosine, sine, ag, mg, kul, kub, vul, vub, wol, wob, gw, uw, dw, out,
+    grid, shapes, res_in, qlt, qbt, lat, cosine, sine, ag, mg, kul, kub, vul, vub, wol_in, wob_in, gw, uw, dw, out,
     lat_all, gate_all, up_all, down_all, ql, qb, ktl, ktb, valt_l, valt_b, peak, total, acc_l, acc_b, att, term, inbox, kept,
-    normed, hidden, inbox2, lat_recv, lat_send, lat_pair, recv, send, own_sem, pair_send, pair_recv,
+    normed, hidden, inbox2, wol, wob, res, lat_recv, lat_send, lat_pair, recv, send, own_sem, pair_send, pair_recv,
 ):
     wide_z, wide_y, wide_x = grid
     n_sp = wide_z * wide_y * wide_x
@@ -340,7 +340,11 @@
     own = [pltpu.make_async_copy(lat, lat_all.at[me], own_sem.at[0])]
     for p, (_, src, at) in enumerate(parts):
         own.append(pltpu.make_async_copy(src, at(me), own_sem.at[1 + p]))
-    for copy in own:
+    fetch = [
+        pltpu.make_async_copy(src, dst, own_sem.at[1 + len(parts) + k])
+        for k, (src, dst) in enumerate(((wol_in, wol), (wob_in, wob), (res_in, res)))
+    ]
+    for copy in own + fetch:
         copy.start()
 
     def send_own(w):
@@ -386,18 +390,28 @@
 
         return 0
 
-    def part_event(n, _):
+    def part_event(n, group):
         origin, valid = origin_of(n)
 
         @pl.when(valid)
         def _():
             i = index_of(origin)
-            for p, (order, _, _) in enumerate(parts):
+            for p in group:
                 part_copy(p, 0, i, False).wait_recv()
                 for w, way in enumerate(ways):
-                    run(wanted(order, origin, way), lambda p=p, w=w: part_copy(p, w, i, False).start())
-
-        return 0
+                    run(
+                        wanted(parts[p][0], origin, way),
+                        lambda p=p, w=w: part_copy(p, w, i, False).start(),
+                    )
+
+    def events(low, high, group):
+        def body(n, _):
+            part_event(n, group)
+            return 0
+
+        lax.fori_loop(low, high, body, 0)
+
+    soon, late = (0, 1, 4, 5), (2, 3)
 
     count = len(table)
     early = sum(1 for dz, fy, fx in table if abs(dz) + fy + fx <= 2)
@@ -469,7 +483,7 @@
             )
 
     def step(j, _):
-        lax.fori_loop((j * early) // n_sp, ((j + 1) * early) // n_sp, part_event, 0)
+        events((j * early) // n_sp, ((j + 1) * early) // n_sp, soon)
         pl.when(j < me)(lambda: attend_block(j, False))
         return 0
 
@@ -490,6 +504,9 @@
     features = out.shape[1]
     block = math.gcd(features, 512)
 
+    for copy in fetch:
+        copy.wait()
+
     def project(n, _):
         cols = pl.ds(pl.multiple_of(n * block, block), block)
         term[:, cols] = (
@@ -526,7 +543,15 @@
     lax.fori_loop(0, share // rows_at_once, norms, 0)
     rows_out = to_pair(1, normed.at[mine], normed.at[mine])
     rows_out.start()
-    lax.fori_loop(early, count, part_event, 0)
+    behind = min(early, count - early)
+
+    def both_groups(n, _):
+        part_event(n, soon)
+        part_event(n - behind, late)
+        return 0
+
+    events(0, early - behind, late)
+    lax.fori_loop(early, count, both_groups, 0)
     to_pair(1, normed.at[theirs], normed.at[theirs]).wait_recv()
 
     def feed(cols):
@@ -535,12 +560,15 @@
         hidden[:, cols] = (gate / (1.0 + jnp.exp(-gate)) * up).astype(bf16)
 
     span = 256
+    chunks = units // span
+    left = count - behind
 
     def feed_loop(n, _):
+        events(left + (n * behind) // chunks, left + ((n + 1) * behind) // chunks, late)
         feed(pl.ds(pl.multiple_of(n * span, span), span))
         return 0
 
-    lax.fori_loop(0, units // span, feed_loop, 0)
+    lax.fori_loop(0, chunks, feed_loop, 0)
     if units % span:
         feed(pl.ds(units // span * span, units % span))
     heads_out.wait_send()
@@ -619,7 +647,9 @@
     return pl.pallas_call(
         functools.partial(layer_kernel, grid, (tokens, share, rope)),
         out_shape=jax.ShapeDtypeStruct((share, features), bf16),
-        in_specs=[vmem] * len(args),
+        in_specs=[
+            pl.BlockSpec(memory_space=pl.ANY) if k in (0, 12, 13) else vmem for k in range(len(args))
+        ],
         out_specs=vmem,
         scratch_shapes=[
             pltpu.VMEM((n_sp, tokens + rope, rank), bf16),
@@ -643,12 +673,15 @@
             pltpu.VMEM((tokens, features), bf16),
             pltpu.VMEM((tokens, units), bf16),
             pltpu.VMEM((share, features), bf16),
+            pltpu.VMEM(wol.shape, bf16),
+            pltpu.VMEM(wob.shape, bf16),
+            pltpu.VMEM(residual_in.shape, bf16),
             dma((n_sp,)),
             dma((4, n_sp)),
             dma((2, n_sp)),
             dma((6, n_sp)),
             dma((6, 4, n_sp)),
-            dma((7,)),
+            dma((10,)),
             dma((3,)),
             dma((3,)),
         ],
@@ -669,7 +702,7 @@
     wide_l, wide_b = args[6].shape[2], args[7].shape[2]
     rope = args[4].shape[1]
     return (
-        tokens % 128 == 0 and tokens <= 256 and share % 16 == 0 and units % 128 == 0
+        tokens % 128 == 0 and tokens <= 256 and share % 16 == 0 and units >= 256
         and units % 64 == 0 and heads_l % 2 == 0 and 2 * wide_l == wide_b and wide_b % 128 == 0
         and args[3].shape[1] == tokens and rope % 32 == 0 and (tokens + rope) % 32 == 0
         and heads_b > 0 and args[8].shape[2] == wide_l and args[9].shape[2] == wide_b

time: 171 us -> 170 us (level)
  Pallas kernels: 161 us -> 159 us
    pallas_call x1, Pallas kernels: 161 us -> 159 us  [fused_shards(): pl.pallas_call(functools.partial(layer_kernel, grid, (tokens, share, rope...]
where the time goes in v3:
time: 170 us; the launch traced here: 169 us
  Pallas kernels  159 us (94%)
  local copies, waits for them, and re-layouts  5.5 us (3%)
  other arithmetic  4.35 us (3%)
    pallas_call x1, Pallas kernels, fused_shards(): pl.pallas_call(functools.partial(layer_kernel, grid, (tokens, share, rope...  159 us
    unnamed x3, local copies, waits for them, and re-layouts  5.5 us

profile of v3, /device:TPU:29, one launch (start us, length us, event | category | flops | bytes accessed | tf_op | source)
XLA Modules:
  0.0 168.7 jit_solution(6159135581782157020)
XLA Ops:
  0.0 1.0 fusion
  1.1 0.7 convert_element_type.24
  1.8 0.1 fusion.8
  1.9 0.8 multiply_sine_fusion
  2.7 1.0 fusion.2
  3.7 0.7 pad_maximum_fusion.lat
  4.4 1.8 %copy.18 = bf16[256,4,128]{0,2,1:T(8,128)(2,1)} copy(bf16[256,4,128]{2,1,0:T(4,128)(2,1)} %param.24) | data formatting | bytes 524288 | tf_op args[7]
  6.2 1.8 %copy.19 = bf16[256,4,128]{0,2,1:T(8,128)(2,1)} copy(bf16[256,4,128]{2,1,0:T(4,128)(2,1)} %param.26) | data formatting | bytes 524288 | tf_op args[9]
  8.0 158.8 %shard_map.163 = bf16[128,2048]{1,0:T(8,128)(2,1)} custom-call(bf16[128,2048]{1,0:T(8,128)(2,1)} %res_in.1, bf16[4,96,256]{2,1,0:T(8,128)(2,1)} %bitcast.25, bf16[4,160,256]{2,1,0:T(8,128)(2,1)} %bitcast.24, bf16[288,256]{1,0:T(8,128)(2,1)} %pad_maximum_fusion.lat, f32[16,256]{1,0:T(8,128)} %get-tuple-element.8.cosine, f32[16,256]{1,0:T(8,128)} %get-tuple-element.7.sine, ...), custom_call_target="tpu_custom_call" | custom-call | tf_op jit(solution)/shard_map/pallas_call | solution.py:647
  166.8 1.9 %copy.21 = bf16[128,2048]{1,0:T(8,128)(2,1)} copy(bf16[128,2048]{1,0:T(8,128)(2,1)} %shard_map.163) | data formatting | bytes 1048576
  (4 shorter events, 0.0 us)
